TPU v7x, 32 devices: a whole 2x2x4 slice. The times are simulated.
32 devices in a mesh: ra: 4 (over z), cb: 4 (over y, x), dp: 2 (over core).
Axes of the slice: x: 2, y: 2, z: 4, core: 2. Of those that a mesh axis runs over, the one named last changes fastest.
Arguments:
- carried: bfloat16 [3072, 4096], P('dp', 'ra'), may hold values from -100 to 100
- branch_in: bfloat16 [3072, 4096], P('dp', 'ra'), may hold values from -12 to 12
- gain_in: float32 [4096], P('ra'), may hold values from 0.1 to 1.9
- bias_in: float32 [4096], P('ra'), may hold values from -1.8 to 1.8
- up_weight: bfloat16 [4096, 16384], P('ra', 'cb'), may hold values from -0.125 to 0.125
- down_weight: bfloat16 [16384, 4096], P('cb', 'ra'), may hold values from -0.046875 to 0.046875
- gain_out: float32 [4096], P('ra'), may hold values from 0.1 to 1.9
- bias_out: float32 [4096], P('ra'), may hold values from -1.8 to 1.8
Outputs:
- layer_out: bfloat16 [3072, 4096], P('dp', 'ra')
All inputs are finite; a program needn't handle non-finite values.
Results may differ from a plain program's by a relative error of at most 0.006.
Values may be sent and summed in bfloat16 or wider, within the bound.
A program may use at most 128 MiB of HBM per device.

v0:
```python
import functools
import math

import jax
import jax.numpy as jnp
from jax import lax
from jax.experimental import pallas as pl
from jax.experimental.pallas import tpu as pltpu
from jax.sharding import PartitionSpec as P

residual_scale = 2.0**0.25
norm_eps = 1e-05
lookahead = 4


def kernel(n, m, nd, block, carried_hbm, branch_hbm, w1_hbm, w2_hbm, gain_in_ref, bias_in_ref,
           gain_ref, bias_ref, o_hbm, s1_src, s1_recv, s1_tot, s1_send, s1_rcv, xall, w1s, h, w2, part, rs_src, rs_recv, mixed, st_src, st_recv, fin,
           loc_sem, w1_send, w1_recv, dp_send, dp_recv, xz_r, xz_l, xz_recv,
           xy_send, xy_recv, h_r, h_l, h_recv, rs_send, rs_rcv, st_send, st_rcv,
           fin_send, fin_rcv):
    me, cb, dp = lax.axis_index("ra"), lax.axis_index("cb"), lax.axis_index("dp")
    _, tokens, dl = xall.shape
    fs = w1s.shape[2]
    blocks = tokens // block
    quarter = tokens // m
    rows = block // m
    half = dl // nd
    pieces = w1_send.shape[1]
    piece = half // pieces
    width = n * dl
    tile = math.gcd(256, math.gcd(fs, dl))

    barrier = pltpu.get_barrier_semaphore()
    for o in range(1, n):
        pl.semaphore_signal(barrier, inc=1, device_id={"ra": lax.rem(me + o, n)})
    for o in range(1, m):
        pl.semaphore_signal(barrier, inc=1, device_id={"cb": lax.rem(cb + o, m)})
    for o in range(1, nd):
        pl.semaphore_signal(barrier, inc=1, device_id={"dp": lax.rem(dp + o, nd)})

    own_carried = pltpu.make_async_copy(carried_hbm, fin, loc_sem.at[0])
    own_branch = pltpu.make_async_copy(branch_hbm, rs_src, loc_sem.at[4])
    own_w1 = pltpu.make_async_copy(
        w1_hbm.at[:, pl.ds(pl.multiple_of(me * fs, fs), fs)], w1s.at[me], loc_sem.at[1])
    own_w2 = pltpu.make_async_copy(w2_hbm, w2, loc_sem.at[2])
    own_carried.start()
    own_branch.start()
    own_w1.start()
    own_w2.start()
    pl.semaphore_wait(barrier, n + m + nd - 3)

    def at_rows(start, size):
        return pl.ds(pl.multiple_of(start, size), size)

    def line(ref_of, right_sem, left_sem, recv_sem, src, to_right):
        ref = ref_of(src)
        return pltpu.make_async_remote_copy(
            src_ref=ref, dst_ref=ref,
            send_sem=(right_sem if to_right else left_sem)(src),
            recv_sem=recv_sem(src),
            device_id={"ra": jnp.minimum(me + 1, n - 1) if to_right else jnp.maximum(me - 1, 0)})

    def start_own(make):
        @pl.when(me + 1 < n)
        def _():
            make(me, True).start()

        @pl.when(me >= 1)
        def _():
            make(me, False).start()

    def relay(make, landed, between=None):
        for s in range(1, n):
            @pl.when(me - s >= 0)
            def _():
                make(me - s, True).wait_recv()

                @pl.when(me + 1 < n)
                def _():
                    make(me - s, True).start()
                landed(me - s)

            @pl.when(me + s < n)
            def _():
                make(me + s, False).wait_recv()

                @pl.when(me >= 1)
                def _():
                    make(me + s, False).start()
                landed(me + s)
            if between is not None:
                between(s)

    def line_sent(make):
        for s in range(n):
            @pl.when((me - s >= 0) & (me + 1 < n))
            def _():
                make(me - s, True).wait_send()

            @pl.when((me + s < n) & (me >= 1))
            def _():
                make(me + s, False).wait_send()

    make_x = functools.partial(
        line, lambda s: xall.at[s, at_rows(cb * quarter, quarter)],
        lambda s: xz_r.at[s], lambda s: xz_l.at[s], lambda s: xz_recv.at[s])

    def xy_copy(src, o):
        ref = xall.at[src, at_rows(cb * quarter, quarter)]
        return pltpu.make_async_remote_copy(
            src_ref=ref, dst_ref=ref, send_sem=xy_send.at[src, o], recv_sem=xy_recv.at[src, cb],
            device_id={"cb": lax.rem(cb + o, m)})

    def xy_landed(src, o):
        sender = lax.rem(cb + o, m)
        ref = xall.at[src, at_rows(sender * quarter, quarter)]
        return pltpu.make_async_remote_copy(
            src_ref=ref, dst_ref=ref, send_sem=xy_send.at[src, o], recv_sem=xy_recv.at[src, sender],
            device_id={"cb": sender})

    def w1_copy(o, p):
        to = lax.rem(me + o, n)
        here = at_rows(dp * half + p * piece, piece)
        return pltpu.make_async_remote_copy(
            src_ref=w1_hbm.at[here, pl.ds(pl.multiple_of(to * fs, fs), fs)],
            dst_ref=w1s.at[me, here],
            send_sem=w1_send.at[to, p], recv_sem=w1_recv.at[me, p], device_id={"ra": to})

    def w1_landed(o, p):
        src = lax.rem(me + o, n)
        ref = w1s.at[src, at_rows(dp * half + p * piece, piece)]
        return pltpu.make_async_remote_copy(
            src_ref=ref, dst_ref=ref, send_sem=w1_send.at[src, p], recv_sem=w1_recv.at[src, p],
            device_id={"ra": src})

    def w1_pieces(p):
        if p < pieces:
            for o in range(1, n):
                w1_copy(o, p).start()

    def s1_copy(o):
        return pltpu.make_async_remote_copy(
            src_ref=s1_src, dst_ref=s1_recv.at[me], send_sem=s1_send.at[o],
            recv_sem=s1_rcv.at[me], device_id={"ra": lax.rem(me + o, n)})

    def s1_landed(o):
        sender = lax.rem(me + o, n)
        ref = s1_recv.at[sender]
        return pltpu.make_async_remote_copy(
            src_ref=ref, dst_ref=ref, send_sem=s1_send.at[o], recv_sem=s1_rcv.at[sender],
            device_id={"ra": sender})

    chunks = tokens // 128

    def mixed_in(here):
        return residual_scale * fin[here, :].astype(jnp.float32) + rs_src[here, :].astype(
            jnp.float32)

    def sums_of(total):
        lane = lax.broadcasted_iota(jnp.int32, (total.shape[0], 128), 1)
        tile = jnp.where(
            lane < 64, jnp.sum(total, axis=1, keepdims=True),
            jnp.sum(total * total, axis=1, keepdims=True))
        if total.shape[0] < 128:
            tile = jnp.concatenate([tile] * (128 // total.shape[0]), axis=0)
        return tile.T

    def column(row):
        return jnp.broadcast_to(row, (128, 128)).T[:, 0:1]

    def dp_copy(o, p):
        src = lax.rem(me + o, n)
        ref = w1s.at[src, at_rows(dp * half, half)]
        return pltpu.make_async_remote_copy(
            src_ref=ref, dst_ref=ref, send_sem=dp_send.at[src, p], recv_sem=dp_recv.at[src, dp],
            device_id={"dp": lax.rem(dp + p, nd)})

    def dp_landed(o, p):
        src = lax.rem(me + o, n)
        sender = lax.rem(dp + p, nd)
        ref = w1s.at[src, at_rows(sender * half, half)]
        return pltpu.make_async_remote_copy(
            src_ref=ref, dst_ref=ref, send_sem=dp_send.at[src, p], recv_sem=dp_recv.at[src, sender],
            device_id={"dp": sender})

    w1_pieces(0)
    own_carried.wait()
    own_branch.wait()

    @pl.loop(0, chunks)
    def _(c):
        sums = sums_of(mixed_in(at_rows(c * 128, 128)))
        s1_src[pl.ds(c, 1), :] = sums[0:1, :]
        s1_src[pl.ds(chunks + c, 1), :] = sums[64:65, :]
    for o in range(1, n):
        s1_copy(o).start()
    s1_tot[...] = s1_src[...]
    for o in range(1, n):
        s1_landed(o).wait_recv()
        s1_tot[...] += s1_recv[lax.rem(me + o, n)]

    @pl.loop(0, chunks)
    def _(c):
        here = at_rows(c * 128, 128)
        mean_row = s1_tot[pl.ds(c, 1), :] / width
        scale_row = lax.rsqrt(s1_tot[pl.ds(chunks + c, 1), :] / width - mean_row * mean_row + norm_eps)
        xall[me, here, :] = (
            (mixed_in(here) - column(mean_row)) * column(scale_row) * gain_in_ref[...]
            + bias_in_ref[...]
        ).astype(jnp.bfloat16)
    start_own(make_x)
    w1_pieces(1)

    def x_landed(src):
        for o in range(1, m):
            xy_copy(src, o).start()

    relay(make_x, x_landed, lambda s: w1_pieces(s + 1))
    for p in range(n + 1, pieces):
        w1_pieces(p)
    for o in range(1, n):
        for p in range(pieces):
            w1_landed(o, p).wait_recv()
        for p in range(1, nd):
            dp_copy(o, p).start()
    own_w1.wait()
    own_w2.wait()
    for o in range(1, n):
        for q in range(1, m):
            xy_landed(lax.rem(me + o, n), q).wait_recv()
        for p in range(1, nd):
            dp_landed(o, p).wait_recv()

    def make_h(b):
        return functools.partial(
            line, lambda s: h.at[s, at_rows(b * block, block)],
            lambda s: h_r.at[b, s], lambda s: h_l.at[b, s], lambda s: h_recv.at[b, s])

    def rs_copy(b, o):
        to = lax.rem(cb + o, m)
        return pltpu.make_async_remote_copy(
            src_ref=rs_src.at[at_rows(b * block + to * rows, rows)], dst_ref=rs_recv.at[b, cb],
            send_sem=rs_send.at[b, o], recv_sem=rs_rcv.at[b, cb], device_id={"cb": to})

    def rs_landed(b, o):
        sender = lax.rem(cb + o, m)
        ref = rs_recv.at[b, sender]
        return pltpu.make_async_remote_copy(
            src_ref=ref, dst_ref=ref, send_sem=rs_send.at[b, o], recv_sem=rs_rcv.at[b, sender],
            device_id={"cb": sender})

    def st_copy(b, o):
        return pltpu.make_async_remote_copy(
            src_ref=st_src.at[b], dst_ref=st_recv.at[b, me],
            send_sem=st_send.at[b, o], recv_sem=st_rcv.at[b, me],
            device_id={"ra": lax.rem(me + o, n)})

    def st_landed(b, o):
        sender = lax.rem(me + o, n)
        ref = st_recv.at[b, sender]
        return pltpu.make_async_remote_copy(
            src_ref=ref, dst_ref=ref, send_sem=st_send.at[b, o], recv_sem=st_rcv.at[b, sender],
            device_id={"ra": sender})

    def fin_copy(b, o):
        ref = fin.at[at_rows(b * block + cb * rows, rows)]
        return pltpu.make_async_remote_copy(
            src_ref=ref, dst_ref=ref, send_sem=fin_send.at[b, o], recv_sem=fin_rcv.at[b, cb],
            device_id={"cb": lax.rem(cb + o, m)})

    def fin_landed(b, o):
        sender = lax.rem(cb + o, m)
        ref = fin.at[at_rows(b * block + sender * rows, rows)]
        return pltpu.make_async_remote_copy(
            src_ref=ref, dst_ref=ref, send_sem=fin_send.at[b, o], recv_sem=fin_rcv.at[b, sender],
            device_id={"cb": sender})

    def up(b):
        here = at_rows(b * block, block)

        @pl.loop(0, fs // tile)
        def _(t):
            cols = at_rows(t * tile, tile)
            acc = jnp.dot(xall[0, here, :], w1s[0, :, cols], preferred_element_type=jnp.float32)
            for k in range(1, n):
                acc += jnp.dot(xall[k, here, :], w1s[k, :, cols], preferred_element_type=jnp.float32)
            h[me, here, cols] = jnp.square(jnp.maximum(acc, 0.0)).astype(jnp.bfloat16)
        start_own(make_h(b))

    def down(b):
        here = at_rows(b * block, block)
        relay(make_h(b), lambda src: None)

        @pl.loop(0, dl // tile)
        def _(t):
            cols = at_rows(t * tile, tile)
            acc = jnp.dot(h[0, here, :], w2[pl.ds(0, fs), cols], preferred_element_type=jnp.float32)
            for k in range(1, n):
                acc += jnp.dot(h[k, here, :], w2[pl.ds(k * fs, fs), cols],
                               preferred_element_type=jnp.float32)
            part[:, cols] = acc
            rs_src[here, cols] = acc.astype(jnp.bfloat16)
        for o in range(1, m):
            rs_copy(b, o).start()
        mixed[b] = part[at_rows(cb * rows, rows), :] + residual_scale * xall[
            me, at_rows(b * block + cb * rows, rows), :].astype(jnp.float32)

    def reduce(b):
        total = mixed[b]
        for o in range(1, m):
            rs_landed(b, o).wait_recv()
            total += rs_recv[b, lax.rem(cb + o, m)].astype(jnp.float32)
        mixed[b] = total
        sums = sums_of(total)
        st_src[b] = jnp.concatenate([sums[0:4, :], sums[64:68, :]], axis=0)
        for o in range(1, n):
            st_copy(b, o).start()

    def finish(b):
        sums = st_src[b]
        for o in range(1, n):
            st_landed(b, o).wait_recv()
            sums += st_recv[b, lax.rem(me + o, n)]
        mean_row = sums[0:1, :] / width
        scale_row = lax.rsqrt(sums[4:5, :] / width - mean_row * mean_row + norm_eps)
        mean, scale = column(mean_row)[0:rows], column(scale_row)[0:rows]
        fin[at_rows(b * block + cb * rows, rows), :] = (
            (mixed[b] - mean) * scale * gain_ref[...] + bias_ref[...]
        ).astype(jnp.bfloat16)
        for o in range(1, m):
            fin_copy(b, o).start()

    @pl.loop(0, blocks + lookahead + 2)
    def _(step):
        for lag, stage in ((0, up), (lookahead, down), (lookahead + 1, reduce),
                           (lookahead + 2, finish)):
            @pl.when((step >= lag) & (step < blocks + lag))
            def _():
                stage(step - lag)

    @pl.loop(0, blocks)
    def _(b):
        for o in range(1, m):
            fin_landed(b, o).wait_recv()
    out = pltpu.make_async_copy(fin, o_hbm, loc_sem.at[3])
    out.start()
    line_sent(make_x)
    for o in range(1, n):
        s1_copy(o).wait_send()
        for p in range(pieces):
            w1_copy(o, p).wait_send()
        for q in range(1, m):
            xy_copy(lax.rem(me + o, n), q).wait_send()
        for p in range(1, nd):
            dp_copy(o, p).wait_send()

    @pl.loop(0, blocks)
    def _(b):
        line_sent(make_h(b))
        for o in range(1, m):
            rs_copy(b, o).wait_send()
            fin_copy(b, o).wait_send()
        for o in range(1, n):
            st_copy(b, o).wait_send()
    out.wait()


def per_device(carried, branch_in, gain_in, bias_in, up_weight, down_weight, gain_out, bias_out):
    n, m, nd = lax.axis_size("ra"), lax.axis_size("cb"), lax.axis_size("dp")
    tokens, dl = carried.shape
    fl = up_weight.shape[1]
    fs = fl // n
    block = math.gcd(tokens, 128)
    blocks = tokens // block
    rows = block // m
    pieces = 4
    chunk_rows = -(-2 * (tokens // 128) // 8) * 8
    dma = pltpu.SemaphoreType.DMA
    bf16, f32 = jnp.bfloat16, jnp.float32
    hbm = pl.BlockSpec(memory_space=pl.ANY)
    vmem = pl.BlockSpec(memory_space=pltpu.VMEM)
    return pl.pallas_call(
        functools.partial(kernel, n, m, nd, block),
        out_shape=jax.ShapeDtypeStruct((tokens, dl), bf16),
        in_specs=[hbm, hbm, hbm, hbm, vmem, vmem, vmem, vmem],
        out_specs=hbm,
        scratch_shapes=[
            pltpu.VMEM((chunk_rows, 128), f32),
            pltpu.VMEM((n, chunk_rows, 128), f32),
            pltpu.VMEM((chunk_rows, 128), f32),
            dma((n,)), dma((n,)),
            pltpu.VMEM((n, tokens, dl), bf16),
            pltpu.VMEM((n, dl, fs), bf16),
            pltpu.VMEM((n, tokens, fs), bf16),
            pltpu.VMEM((fl, dl), bf16),
            pltpu.VMEM((block, dl), f32),
            pltpu.VMEM((tokens, dl), bf16),
            pltpu.VMEM((blocks, m, rows, dl), bf16),
            pltpu.VMEM((blocks, rows, dl), f32),
            pltpu.VMEM((blocks, 8, 128), f32),
            pltpu.VMEM((blocks, n, 8, 128), f32),
            pltpu.VMEM((tokens, dl), bf16),
            dma((5,)), dma((n, pieces)), dma((n, pieces)), dma((n, nd)), dma((n, nd)),
            dma((n,)), dma((n,)), dma((n,)), dma((n, m)), dma((n, m)),
            dma((blocks, n)), dma((blocks, n)), dma((blocks, n)),
            dma((blocks, m)), dma((blocks, m)), dma((blocks, n)), dma((blocks, n)),
            dma((blocks, m)), dma((blocks, m)),
        ],
        compiler_params=pltpu.CompilerParams(
            collective_id=0, has_side_effects=True, vmem_limit_bytes=66 * 1000 * 1000),
    )(carried, branch_in, up_weight, down_weight, gain_in.reshape(1, dl), bias_in.reshape(1, dl),
      gain_out.reshape(1, dl), bias_out.reshape(1, dl))


def solution(mesh):
    in_specs = (
        P("dp", "ra"),
        P("dp", "ra"),
        P("ra"),
        P("ra"),
        P("ra", "cb"),
        P("cb", "ra"),
        P("ra"),
        P("ra"),
    )
    out_specs = P("dp", "ra")
    return jax.shard_map(
        per_device, mesh=mesh, in_specs=in_specs, out_specs=out_specs, check_vma=False
    )
```

profile of v0, /device:TPU:0, one launch (start us, length us, event | category | flops | bytes accessed | tf_op | source)
XLA Modules:
  0.0 387.8 jit_solution(10451540366887437405)
XLA Ops:
  0.0 384.0 %shard_map.82 = bf16[1536,1024]{1,0:T(8,128)(2,1)} custom-call(bf16[1536,1024]{1,0:T(8,128)(2,1)} %carried_hbm.1, bf16[1536,1024]{1,0:T(8,128)(2,1)} %branch_hbm.1, bf16[1024,4096]{1,0:T(8,128)(2,1)} %w1_hbm.1, bf16[4096,1024]{1,0:T(8,128)(2,1)} %w2_hbm.1, f32[1,1024]{1,0:T(1,128)} %bitcast.4, f32[1,1024]{1,0:T(1,128)} %bitcast.5, f32[1,1024]{1,0:T(1,128)} %bitcast.6, ...), custom_call_target="tpu_custom_call" | custom-call | tf_op jit(solution)/shard_map/pallas_call | solution.py:382
  384.0 3.9 copy.10
where the time goes:
time: 388 us
  Pallas kernels  384 us (99%)
    pallas_call x1, Pallas kernels, per_device(): pl.pallas_call(functools.partial(kernel, n, m, nd, block), out_shape=jax....  384 us

commit v1 on v0

v1 whole, which is shorter than its diff:
```python
import functools
import math

import jax
import jax.numpy as jnp
from jax import lax
from jax.experimental import pallas as pl
from jax.experimental.pallas import tpu as pltpu
from jax.sharding import PartitionSpec as P

residual_scale = 2.0**0.25
norm_eps = 1e-05
tile_cap = 256
lag_x, lag_a, lag_z = 2, 4, 6
lead = 2


def kernel(n, m, tile, carried_hbm, branch_hbm, w1_hbm, w2_hbm, gain_in_ref, bias_in_ref, gain_ref,
           bias_ref, o_hbm, s1_src, s1_recv, s1_tot, xh, xres, w1s, w2s, h, psend, yrecv, zsend,
           zrecv, fin, acc, st_src, st_recv, loc_sem, s1_sem, w1_sem, w2_sem, xz_sem, xy_sem,
           y_sem, z_sem, ag_sem, st_send, st_rcv, out_sem):
    me, cb, dp = lax.axis_index("ra"), lax.axis_index("cb"), lax.axis_index("dp")
    tokens, dl = xres.shape
    fs = h.shape[2]
    q = tokens // m
    chunks = tokens // 128
    qchunks = q // 128
    rounds1, rounds2 = fs // tile, dl // tile
    tiles = rounds2 * n
    width = n * dl
    xb, yb = lax.rem(cb, 2), cb // 2
    px, py = cb + 1 - 2 * xb, lax.rem(cb + 2, m)
    sib = 1 - dp

    def slot_of(c):
        return lax.rem(c, 2) * 2 + c // 2

    def at_rows(start, size):
        return pl.ds(pl.multiple_of(start, size), size)

    def remote(src, dst, send, recv, to):
        return pltpu.make_async_remote_copy(
            src_ref=src, dst_ref=dst, send_sem=send, recv_sem=recv, device_id=to)

    barrier = pltpu.get_barrier_semaphore()
    for o in range(n):
        for c in range(m):
            if o or c:
                pl.semaphore_signal(barrier, inc=1, device_id={
                    "ra": lax.rem(me + o, n), "cb": lax.rem(cb + c, m)})
    pl.semaphore_signal(barrier, inc=1, device_id={"dp": sib})

    own_carried = pltpu.make_async_copy(carried_hbm, fin, loc_sem.at[0])
    own_branch = pltpu.make_async_copy(branch_hbm, psend.at[pl.ds(0, tokens)], loc_sem.at[1])
    own_w1 = pltpu.make_async_copy(w1_hbm.at[:, at_rows(me * fs, fs)], w1s.at[0, me], loc_sem.at[2])
    own_w2 = pltpu.make_async_copy(w2_hbm.at[at_rows(me * fs, fs)], w2s.at[0, me], loc_sem.at[3])
    own_carried.start()
    own_branch.start()
    own_w1.start()
    own_w2.start()
    pl.semaphore_wait(barrier, n * m)

    class Stream:
        def __init__(self, buf, sem, block):
            self.buf, self.sem, self.block = buf, sem, block
            half = buf.shape[2] // 2
            self.rows = at_rows(dp * half, half)
            self.other = at_rows(sib * half, half)

        def ref(self, share, src, p, rows):
            return self.buf.at[share, src, rows, at_rows(p * tile, tile)]

        def z(self, to, p):
            return remote(self.block(to, p), self.ref(0, me, p, self.rows),
                          self.sem.at[0, to, p], self.sem.at[1, me, p], {"ra": to})

        def z_landed(self, src, p):
            ref = self.ref(0, src, p, self.rows)
            return remote(ref, ref, self.sem.at[0, src, p], self.sem.at[1, src, p], {"ra": src})

        def x(self, src, p):
            ref = self.ref(0, src, p, self.rows)
            return remote(ref, self.ref(1, src, p, self.rows), self.sem.at[2, src, p],
                          self.sem.at[3, src, p], {"cb": px})

        def x_own(self, p):
            return remote(self.block(me, p), self.ref(1, me, p, self.rows), self.sem.at[2, me, p],
                          self.sem.at[3, me, p], {"cb": px})

        def pair(self, share, src, p):
            ref = self.ref(share, src, p, self.rows)
            return remote(ref, ref, self.sem.at[4 + 2 * share, src, p],
                          self.sem.at[5 + 2 * share, src, p], {"dp": sib})

        def pair_landed(self, share, src, p):
            ref = self.ref(share, src, p, self.other)
            return remote(ref, ref, self.sem.at[4 + 2 * share, src, p],
                          self.sem.at[5 + 2 * share, src, p], {"dp": sib})

        def send(self, p, least=1, most=n - 1):
            for o in range(least, most + 1):
                @pl.when(me + o < n)
                def _():
                    self.z(me + o, p).start()

                @pl.when(me >= o)
                def _():
                    self.z(me - o, p).start()

        def forward(self, src, p):
            @pl.when(src != me)
            def _():
                self.z_landed(src, p).wait_recv()
                self.x(src, p).start()
                self.pair(0, src, p).start()

        def forward_near(self, p):
            for o in range(1, n):
                @pl.when(me + o < n)
                def _():
                    self.forward(me + o, p)

                @pl.when(me >= o)
                def _():
                    self.forward(me - o, p)

        def share(self, src, p):
            self.x(src, p).wait_recv()
            self.pair(1, src, p).start()

        def ready(self, src, p):
            @pl.when(src != me)
            def _():
                self.pair_landed(0, src, p).wait_recv()
            self.pair_landed(1, src, p).wait_recv()

        def sent(self, src, p):
            @pl.when(src != me)
            def _():
                self.z(src, p).wait_send()
                self.pair(0, src, p).wait_send()
            self.x(src, p).wait_send()
            self.pair(1, src, p).wait_send()

    one = Stream(w1s, w1_sem, lambda to, p: w1_hbm.at[
        at_rows(dp * (dl // 2), dl // 2), at_rows(to * fs + p * tile, tile)])
    two = Stream(w2s, w2_sem, lambda to, p: w2_hbm.at[
        at_rows(to * fs + dp * (fs // 2), fs // 2), at_rows(p * tile, tile)])

    one.send(0, 1, 1)
    for p in range(rounds1):
        one.x_own(p).start()

    def s1_copy(o):
        return remote(s1_src, s1_recv.at[me], s1_sem.at[0, o], s1_sem.at[1, me],
                      {"ra": lax.rem(me + o, n)})

    def s1_landed(o):
        sender = lax.rem(me + o, n)
        ref = s1_recv.at[sender]
        return remote(ref, ref, s1_sem.at[0, o], s1_sem.at[1, sender], {"ra": sender})

    def mixed_in(here):
        return residual_scale * fin[here, :].astype(jnp.float32) + psend[here, :].astype(
            jnp.float32)

    def sums_of(total):
        lane = lax.broadcasted_iota(jnp.int32, (128, 128), 1)
        return jnp.where(
            lane < 64, jnp.sum(total, axis=1, keepdims=True),
            jnp.sum(total * total, axis=1, keepdims=True)).T

    def column(row):
        return jnp.broadcast_to(row, (128, 128)).T[:, 0:1]

    st_src[...] = jnp.zeros_like(st_src)
    own_carried.wait()
    own_branch.wait()

    @pl.loop(0, chunks)
    def _(c):
        sums = sums_of(mixed_in(at_rows(c * 128, 128)))
        s1_src[pl.ds(c, 1), :] = sums[0:1, :]
        s1_src[pl.ds(chunks + c, 1), :] = sums[64:65, :]
    for o in range(1, n):
        s1_copy(o).start()
    if n > 2:
        one.send(0, 2, 2)
    s1_tot[...] = s1_src[...]
    for o in range(1, n):
        s1_landed(o).wait_recv()
        s1_tot[...] += s1_recv[lax.rem(me + o, n)]

    def normed(c):
        mean_row = s1_tot[pl.ds(c, 1), :] / width
        scale_row = lax.rsqrt(s1_tot[pl.ds(chunks + c, 1), :] / width - mean_row * mean_row + norm_eps)
        here = at_rows(c * 128, 128)
        out = ((mixed_in(here) - column(mean_row)) * column(scale_row) * gain_in_ref[...]
               + bias_in_ref[...]).astype(jnp.bfloat16)
        xres[here, :] = out
        return out

    def normed_half(first, count):
        @pl.loop(0, count)
        def _(c):
            local = first + c
            xh[me, at_rows(local * 128, 128), :] = normed(xb * 2 * qchunks + local)

    normed_half(yb * qchunks, qchunks)

    def xz(src, to_right):
        ref = xh.at[src, at_rows(yb * q, q)]
        return remote(ref, ref, xz_sem.at[0 if to_right else 1, src], xz_sem.at[2, src], {
            "ra": jnp.minimum(me + 1, n - 1) if to_right else jnp.maximum(me - 1, 0)})

    def xy(src):
        ref = xh.at[src, at_rows(yb * q, q)]
        return remote(ref, ref, xy_sem.at[0, src], xy_sem.at[1, src], {"cb": py})

    def xy_landed(src):
        ref = xh.at[src, at_rows((1 - yb) * q, q)]
        return remote(ref, ref, xy_sem.at[0, src], xy_sem.at[1, src], {"cb": py})

    def from_left(s):
        @pl.when(me >= s)
        def _():
            xz(me - s, True).wait_recv()

            @pl.when(me + 1 < n)
            def _():
                xz(me - s, True).start()
            xy(me - s).start()

    def from_right(s):
        @pl.when(me + s < n)
        def _():
            xz(me + s, False).wait_recv()

            @pl.when(me >= 1)
            def _():
                xz(me + s, False).start()
            xy(me + s).start()

    @pl.when(me + 1 < n)
    def _():
        xz(me, True).start()

    @pl.when(me >= 1)
    def _():
        xz(me, False).start()
    if n > 3:
        one.send(0, 3)
    if rounds1 > 1:
        one.send(1)
    normed_half((1 - yb) * qchunks, qchunks)

    @pl.loop(0, 2 * qchunks)
    def _(c):
        normed((1 - xb) * 2 * qchunks + c)

    one.forward_near(0)
    two.x_own(0).start()
    for s in range(1, max(n, rounds1)):
        if s < n:
            from_left(s)
            from_right(s)
        if s + 1 < rounds1:
            one.send(s + 1)
        if s < rounds2:
            two.x_own(s).start()
        if s < rounds1 - 1:
            one.forward_near(s)
            for src in range(n):
                one.share(src, s - 1)
    for p in range(n, rounds2):
        two.x_own(p).start()
    for p in range(min(lead, rounds2)):
        two.send(p)

    own_w1.wait()
    for src in range(n):
        @pl.when(src != me)
        def _():
            xy_landed(src).wait_recv()

    def up(p):
        for src in range(n):
            one.ready(src, p)
        cols = at_rows(p * tile, tile)
        for share in range(2):
            @pl.loop(0, 2)
            def _(b):
                here = at_rows(b * q, q)
                total = jnp.dot(xh[0, here, :], w1s[share, 0, :, cols],
                                preferred_element_type=jnp.float32)
                for k in range(1, n):
                    total += jnp.dot(xh[k, here, :], w1s[share, k, :, cols],
                                     preferred_element_type=jnp.float32)
                h[share, here, cols] = jnp.square(jnp.maximum(total, 0.0)).astype(jnp.bfloat16)

    @pl.loop(0, max(rounds1 - 2, 0))
    def _(p):
        up(p)
    if rounds1 > 1:
        one.forward_near(rounds1 - 1)
        for src in range(n):
            one.share(src, rounds1 - 2)
        up(rounds1 - 2)
    for src in range(n):
        one.share(src, rounds1 - 1)
    up(rounds1 - 1)
    own_w2.wait()

    def where_of(t):
        return t // n, lax.rem(t, n)

    def out_tile(ref, block, r):
        return ref.at[at_rows(block * q, q), at_rows(r * tile, tile)]

    def down(start, d, r):
        cols = at_rows(r * tile, tile)
        here = at_rows(start, q)
        return (jnp.dot(h[0, here, :], w2s[0, d, :, cols], preferred_element_type=jnp.float32)
                + jnp.dot(h[1, here, :], w2s[1, d, :, cols], preferred_element_type=jnp.float32))

    def y_copy(t):
        r, d = where_of(t)
        return remote(out_tile(psend, d, r), out_tile(yrecv, d, r), y_sem.at[0, t], y_sem.at[1, t],
                      {"cb": py})

    def z_copy(t, to_right):
        r, d = where_of(t)
        to = jnp.minimum(me + 1, n - 1) if to_right else jnp.maximum(me - 1, 0)
        block = d if to_right else jnp.where(d == to, n, d)
        return remote(out_tile(zsend, d, r), out_tile(zrecv, block, r), z_sem.at[0, t],
                      z_sem.at[1 if to_right else 2, t], {"ra": to})

    def z_landed(t, to_right):
        r, d = where_of(t)
        block = d if to_right else jnp.where(d == me, n, d)
        ref = out_tile(zrecv, block, r)
        return remote(ref, ref, z_sem.at[0, t], z_sem.at[1 if to_right else 2, t], {
            "ra": jnp.maximum(me - 1, 0) if to_right else jnp.minimum(me + 1, n - 1)})

    def ag_copy(r, o):
        ref = out_tile(fin, slot_of(cb), r)
        return remote(ref, ref, ag_sem.at[0, r, o], ag_sem.at[1, r, cb], {"cb": lax.rem(cb + o, m)})

    def ag_landed(r, o):
        sender = lax.rem(cb + o, m)
        ref = out_tile(fin, slot_of(sender), r)
        return remote(ref, ref, ag_sem.at[0, r, o], ag_sem.at[1, r, sender], {"cb": sender})

    def st_copy(o, c):
        return remote(st_src, st_recv.at[me, cb], st_send.at[o, c], st_rcv.at[me, cb],
                      {"ra": lax.rem(me + o, n), "cb": lax.rem(cb + c, m)})

    def st_landed(o, c):
        z, s = lax.rem(me + o, n), lax.rem(cb + c, m)
        ref = st_recv.at[z, s]
        return remote(ref, ref, st_send.at[o, c], st_rcv.at[z, s], {"ra": z, "cb": s})

    def stage_r(t):
        r, d = where_of(t)
        two.forward(d, r)

    def stage_x(t):
        r, d = where_of(t)
        two.share(d, r)

    def stage_a(t):
        r, d = where_of(t)
        two.ready(d, r)
        out_tile(psend, d, r)[...] = down((1 - yb) * q, d, r).astype(jnp.bfloat16)
        y_copy(t).start()

    def stage_z(t):
        r, d = where_of(t)
        acc[...] = down(yb * q, d, r)
        y_copy(t).wait_recv()
        acc[...] += out_tile(yrecv, d, r)[...].astype(jnp.float32)

        @pl.when((me >= 1) & (d >= me))
        def _():
            z_landed(t, True).wait_recv()
            acc[...] += out_tile(zrecv, d, r)[...].astype(jnp.float32)

        @pl.when((me + 1 < n) & (d <= me))
        def _():
            z_landed(t, False).wait_recv()
            acc[...] += out_tile(zrecv, jnp.where(d == me, n, d), r)[...].astype(jnp.float32)

        @pl.when(d != me)
        def _():
            out_tile(zsend, d, r)[...] = acc[...].astype(jnp.bfloat16)

        @pl.when(d > me)
        def _():
            z_copy(t, True).start()

        @pl.when(d < me)
        def _():
            z_copy(t, False).start()

        @pl.when(d == me)
        def _():
            out_tile(fin, slot_of(cb), r)[...] = acc[...].astype(jnp.bfloat16)
            for o in range(1, m):
                ag_copy(r, o).start()
            for c in range(qchunks):
                sums = sums_of(acc[pl.ds(c * 128, 128), :] + residual_scale * xres[
                    at_rows(slot_of(cb) * q + c * 128, 128), at_rows(r * tile, tile)].astype(
                        jnp.float32))
                st_src[pl.ds(c, 1), :] += sums[0:1, :]
                st_src[pl.ds(qchunks + c, 1), :] += sums[64:65, :]

            @pl.when(r == rounds2 - 1)
            def _():
                for o in range(n):
                    for c in range(m):
                        if o or c:
                            st_copy(o, c).start()

    @pl.loop(0, tiles + lag_z + n - 1)
    def _(step):
        for r in range(lead, rounds2):
            @pl.when(step == (r - lead + 1) * n)
            def _():
                two.send(r)
        for lag, stage in ((0, stage_r), (lag_x, stage_x), (lag_a, stage_a)):
            @pl.when((step >= lag) & (step < tiles + lag))
            def _():
                stage(step - lag)

        @pl.loop(0, n)
        def _(back):
            hop = n - 1 - back
            t = step - lag_z - hop
            d = lax.rem(t + n * n, n)
            mine = jnp.where(d > me, me, jnp.where(
                d < me, n - 1 - me, jnp.maximum(me, n - 1 - me)))

            @pl.when((t >= 0) & (t < tiles) & (mine == hop))
            def _():
                stage_z(t)

    for o in range(n):
        for c in range(m):
            if o or c:
                st_landed(o, c).wait_recv()
    st_recv[me, cb] = st_src[...]
    for o in range(1, m):
        for r in range(rounds2):
            ag_landed(r, o).wait_recv()

    def out_copy(c):
        here = at_rows(c * 128, 128)
        return pltpu.make_async_copy(xres.at[here], o_hbm.at[here], out_sem.at[c])

    for slot in range(m):
        owner = slot // 2 + 2 * (slot % 2)
        total = st_recv[0, owner]
        for z in range(1, n):
            total += st_recv[z, owner]
        s1_tot[pl.ds(0, 2 * qchunks), :] = total[0:2 * qchunks, :]

        @pl.loop(0, qchunks)
        def _(c):
            mean_row = s1_tot[pl.ds(c, 1), :] / width
            scale_row = lax.rsqrt(
                s1_tot[pl.ds(qchunks + c, 1), :] / width - mean_row * mean_row + norm_eps)
            here = at_rows(slot * q + c * 128, 128)
            mixed = residual_scale * xres[here, :].astype(jnp.float32) + fin[here, :].astype(
                jnp.float32)
            xres[here, :] = ((mixed - column(mean_row)) * column(scale_row) * gain_ref[...]
                             + bias_ref[...]).astype(jnp.bfloat16)
            out_copy(slot * qchunks + c).start()

    for src in range(n):
        @pl.when((src == me) | (src < me))
        def _():
            @pl.when(me + 1 < n)
            def _():
                xz(src, True).wait_send()

        @pl.when((src == me) | (src > me))
        def _():
            @pl.when(me >= 1)
            def _():
                xz(src, False).wait_send()

        @pl.when(src != me)
        def _():
            xy(src).wait_send()

        for stream, count in ((one, rounds1), (two, rounds2)):
            @pl.loop(0, count)
            def _(p):
                stream.sent(src, p)
    for o in range(1, n):
        s1_copy(o).wait_send()

    @pl.loop(0, tiles)
    def _(t):
        d = lax.rem(t, n)
        y_copy(t).wait_send()

        @pl.when(d != me)
        def _():
            z_copy(t, True).wait_send()

    for o in range(1, m):
        for r in range(rounds2):
            ag_copy(r, o).wait_send()
    for o in range(n):
        for c in range(m):
            if o or c:
                st_copy(o, c).wait_send()

    @pl.loop(0, chunks)
    def _(c):
        out_copy(c).wait()


def per_device(carried, branch_in, gain_in, bias_in, up_weight, down_weight, gain_out, bias_out):
    n, m, nd = lax.axis_size("ra"), lax.axis_size("cb"), lax.axis_size("dp")
    tokens, dl = carried.shape
    fs = up_weight.shape[1] // n
    assert m == 4 and nd == 2 and tokens % (128 * m) == 0 and tokens // m <= 512
    q = tokens // m
    tile = math.gcd(tile_cap, math.gcd(fs, dl))
    rounds1, rounds2 = fs // tile, dl // tile
    tiles = rounds2 * n
    chunk_rows = -(-2 * (tokens // 128) // 8) * 8
    dma = pltpu.SemaphoreType.DMA
    bf16, f32 = jnp.bfloat16, jnp.float32
    hbm = pl.BlockSpec(memory_space=pl.ANY)
    vmem = pl.BlockSpec(memory_space=pltpu.VMEM)
    return pl.pallas_call(
        functools.partial(kernel, n, m, tile),
        out_shape=jax.ShapeDtypeStruct((tokens, dl), bf16),
        in_specs=[hbm, hbm, hbm, hbm, vmem, vmem, vmem, vmem],
        out_specs=hbm,
        scratch_shapes=[
            pltpu.VMEM((chunk_rows, 128), f32),
            pltpu.VMEM((n, chunk_rows, 128), f32),
            pltpu.VMEM((chunk_rows, 128), f32),
            pltpu.VMEM((n, 2 * q, dl), bf16),
            pltpu.VMEM((tokens, dl), bf16),
            pltpu.VMEM((2, n, dl, fs), bf16),
            pltpu.VMEM((2, n, fs, dl), bf16),
            pltpu.VMEM((2, 2 * q, fs), bf16),
            pltpu.VMEM((max(n, m) * q, dl), bf16),
            pltpu.VMEM((n * q, dl), bf16),
            pltpu.VMEM((n * q, dl), bf16),
            pltpu.VMEM(((n + 1) * q, dl), bf16),
            pltpu.VMEM((tokens, dl), bf16),
            pltpu.VMEM((q, tile), f32),
            pltpu.VMEM((8, 128), f32),
            pltpu.VMEM((n, m, 8, 128), f32),
            dma((4,)), dma((2, n)), dma((8, n, rounds1)), dma((8, n, rounds2)), dma((3, n)),
            dma((2, n)), dma((2, tiles)), dma((3, tiles)), dma((2, rounds2, m)), dma((n, m)),
            dma((n, m)), dma((tokens // 128,)),
        ],
        compiler_params=pltpu.CompilerParams(
            collective_id=0, has_side_effects=True, vmem_limit_bytes=67 * 1000 * 1000),
    )(carried, branch_in, up_weight, down_weight, gain_in.reshape(1, dl), bias_in.reshape(1, dl),
      gain_out.reshape(1, dl), bias_out.reshape(1, dl))


def solution(mesh):
    in_specs = (
        P("dp", "ra"),
        P("dp", "ra"),
        P("ra"),
        P("ra"),
        P("ra", "cb"),
        P("cb", "ra"),
        P("ra"),
        P("ra"),
    )
    out_specs = P("dp", "ra")
    return jax.shard_map(
        per_device, mesh=mesh, in_specs=in_specs, out_specs=out_specs, check_vma=False
    )
```

time: 388 us -> 345 us (0.89)
  Pallas kernels: 384 us -> 337 us
    pallas_call x1, Pallas kernels: 384 us -> 337 us  [per_device(): pl.pallas_call(functools.partial(kernel, n, m, tile), out_shape=jax.Shape...]
where the time goes in v1:
time: 345 us; the launch traced here: 341 us
  Pallas kernels  337 us (98%)
  local copies, waits for them, and re-layouts  3.86 us (1%)
    pallas_call x1, Pallas kernels, per_device(): pl.pallas_call(functools.partial(kernel, n, m, tile), out_shape=jax.Shape...  337 us

profile of v1, /device:TPU:0, one launch (start us, length us, event | category | flops | bytes accessed | tf_op | source)
XLA Modules:
  0.0 341.3 jit_solution(8340204264452075267)
XLA Ops:
  0.0 337.4 %shard_map.82 = bf16[1536,1024]{1,0:T(8,128)(2,1)} custom-call(bf16[1536,1024]{1,0:T(8,128)(2,1)} %carried_hbm.1, bf16[1536,1024]{1,0:T(8,128)(2,1)} %branch_hbm.1, bf16[1024,4096]{1,0:T(8,128)(2,1)} %w1_hbm.1, bf16[4096,1024]{1,0:T(8,128)(2,1)} %w2_hbm.1, f32[1,1024]{1,0:T(1,128)} %bitcast.4, f32[1,1024]{1,0:T(1,128)} %bitcast.5, f32[1,1024]{1,0:T(1,128)} %bitcast.6, ...), custom_call_target="tpu_custom_call" | custom-call | tf_op jit(solution)/shard_map/pallas_call | solution.py:539
  337.5 3.9 %copy.10 = bf16[1536,1024]{1,0:T(8,128)(2,1)} copy(bf16[1536,1024]{1,0:T(8,128)(2,1)} %shard_map.82) | data formatting | bytes 6291456

commit v2 on v1

--- a/solution.py
+++ b/solution.py
@@ -11,22 +11,28 @@
 residual_scale = 2.0**0.25
 norm_eps = 1e-05
 tile_cap = 256
-lag_x, lag_a, lag_z = 2, 4, 6
-lead = 2
-
-
-def kernel(n, m, tile, carried_hbm, branch_hbm, w1_hbm, w2_hbm, gain_in_ref, bias_in_ref, gain_ref,
+tile2_cap = 128
+lag_x, lag_a, lag_z, lag_hop, lag_late = 3, 8, 14, 4, 12
+lead = 3
+lead_mid = 5
+near = 3
+early = 2
+lag_g = 1
+
+
+def kernel(n, m, tile, tile2, carried_hbm, branch_hbm, w1_hbm, w2_hbm, gain_in_ref, bias_in_ref, gain_ref,
            bias_ref, o_hbm, s1_src, s1_recv, s1_tot, xh, xres, w1s, w2s, h, psend, yrecv, zsend,
            zrecv, fin, acc, st_src, st_recv, loc_sem, s1_sem, w1_sem, w2_sem, xz_sem, xy_sem,
-           y_sem, z_sem, ag_sem, st_send, st_rcv, out_sem):
+           y_sem, z_sem, ag_sem, st_send, st_rcv, out_sem, meet_sem):
     me, cb, dp = lax.axis_index("ra"), lax.axis_index("cb"), lax.axis_index("dp")
     tokens, dl = xres.shape
     fs = h.shape[2]
     q = tokens // m
     chunks = tokens // 128
     qchunks = q // 128
-    rounds1, rounds2 = fs // tile, dl // tile
+    rounds1, rounds2 = fs // tile, dl // tile2
     tiles = rounds2 * n
+    first = min(early, rounds1)
     width = n * dl
     xb, yb = lax.rem(cb, 2), cb // 2
     px, py = cb + 1 - 2 * xb, lax.rem(cb + 2, m)
@@ -61,14 +67,14 @@
     pl.semaphore_wait(barrier, n * m)
 
     class Stream:
-        def __init__(self, buf, sem, block):
-            self.buf, self.sem, self.block = buf, sem, block
+        def __init__(self, buf, sem, tile, block):
+            self.buf, self.sem, self.tile, self.block = buf, sem, tile, block
             half = buf.shape[2] // 2
             self.rows = at_rows(dp * half, half)
             self.other = at_rows(sib * half, half)
 
         def ref(self, share, src, p, rows):
-            return self.buf.at[share, src, rows, at_rows(p * tile, tile)]
+            return self.buf.at[share, src, rows, at_rows(p * self.tile, self.tile)]
 
         def z(self, to, p):
             return remote(self.block(to, p), self.ref(0, me, p, self.rows),
@@ -97,32 +103,45 @@
             return remote(ref, ref, self.sem.at[4 + 2 * share, src, p],
                           self.sem.at[5 + 2 * share, src, p], {"dp": sib})
 
-        def send(self, p, least=1, most=n - 1):
+        def right(self, p, least, most):
             for o in range(least, most + 1):
                 @pl.when(me + o < n)
                 def _():
                     self.z(me + o, p).start()
 
+        def left(self, p, least, most):
+            for o in range(least, most + 1):
                 @pl.when(me >= o)
                 def _():
                     self.z(me - o, p).start()
 
+        def send(self, p, least=1, most=n - 1):
+            for o in range(least, most + 1):
+                self.right(p, o, o)
+                self.left(p, o, o)
+
         def forward(self, src, p):
-            @pl.when(src != me)
-            def _():
-                self.z_landed(src, p).wait_recv()
-                self.x(src, p).start()
-                self.pair(0, src, p).start()
-
-        def forward_near(self, p):
-            for o in range(1, n):
-                @pl.when(me + o < n)
-                def _():
-                    self.forward(me + o, p)
-
-                @pl.when(me >= o)
-                def _():
-                    self.forward(me - o, p)
+            self.z_landed(src, p).wait_recv()
+            self.x(src, p).start()
+            self.pair(0, src, p).start()
+
+        def forward_from(self, o, p):
+            @pl.when(me + o < n)
+            def _():
+                self.forward(me + o, p)
+
+            @pl.when(me >= o)
+            def _():
+                self.forward(me - o, p)
+
+        def share_from(self, o, p):
+            @pl.when(me + o < n)
+            def _():
+                self.share(me + o, p)
+
+            @pl.when(me >= o)
+            def _():
+                self.share(me - o, p)
 
         def share(self, src, p):
             self.x(src, p).wait_recv()
@@ -142,10 +161,10 @@
             self.x(src, p).wait_send()
             self.pair(1, src, p).wait_send()
 
-    one = Stream(w1s, w1_sem, lambda to, p: w1_hbm.at[
+    one = Stream(w1s, w1_sem, tile, lambda to, p: w1_hbm.at[
         at_rows(dp * (dl // 2), dl // 2), at_rows(to * fs + p * tile, tile)])
-    two = Stream(w2s, w2_sem, lambda to, p: w2_hbm.at[
-        at_rows(to * fs + dp * (fs // 2), fs // 2), at_rows(p * tile, tile)])
+    two = Stream(w2s, w2_sem, tile2, lambda to, p: w2_hbm.at[
+        at_rows(to * fs + dp * (fs // 2), fs // 2), at_rows(p * tile2, tile2)])
 
     one.send(0, 1, 1)
     for p in range(rounds1):
@@ -184,8 +203,8 @@
         s1_src[pl.ds(chunks + c, 1), :] = sums[64:65, :]
     for o in range(1, n):
         s1_copy(o).start()
-    if n > 2:
-        one.send(0, 2, 2)
+    for p in range(1, first):
+        one.send(p, 1, 1)
     s1_tot[...] = s1_src[...]
     for o in range(1, n):
         s1_landed(o).wait_recv()
@@ -241,6 +260,31 @@
                 xz(me + s, False).start()
             xy(me + s).start()
 
+    def meet():
+        pl.semaphore_signal(meet_sem, inc=1, device_id={"dp": sib})
+        pl.semaphore_wait(meet_sem, 1)
+
+    def after_relays(s):
+        @pl.when(me == s)
+        def _():
+            for p in range(first, rounds1):
+                one.right(p, 1, 1)
+
+        @pl.when(me == n - 1 - s)
+        def _():
+            for p in range(first, rounds1):
+                one.left(p, 1, 1)
+        for o in range(2, n):
+            @pl.when(me + o == s)
+            def _():
+                for p in range(rounds1):
+                    one.right(p, o, o)
+
+            @pl.when(me - o == n - 1 - s)
+            def _():
+                for p in range(rounds1):
+                    one.left(p, o, o)
+
     @pl.when(me + 1 < n)
     def _():
         xz(me, True).start()
@@ -248,40 +292,30 @@
     @pl.when(me >= 1)
     def _():
         xz(me, False).start()
-    if n > 3:
-        one.send(0, 3)
-    if rounds1 > 1:
-        one.send(1)
+    after_relays(0)
     normed_half((1 - yb) * qchunks, qchunks)
 
     @pl.loop(0, 2 * qchunks)
     def _(c):
         normed((1 - xb) * 2 * qchunks + c)
 
-    one.forward_near(0)
-    two.x_own(0).start()
-    for s in range(1, max(n, rounds1)):
-        if s < n:
-            from_left(s)
-            from_right(s)
-        if s + 1 < rounds1:
-            one.send(s + 1)
-        if s < rounds2:
-            two.x_own(s).start()
-        if s < rounds1 - 1:
-            one.forward_near(s)
-            for src in range(n):
-                one.share(src, s - 1)
-    for p in range(n, rounds2):
+    for p in range(first):
+        one.forward_from(1, p)
+    for p in range(rounds2):
         two.x_own(p).start()
-    for p in range(min(lead, rounds2)):
-        two.send(p)
+    for s in range(1, n):
+        from_left(s)
+        from_right(s)
+        meet()
+        after_relays(s)
+    for p in range(min(near, rounds2)):
+        two.send(p, 1, 1)
+    for p in range(rounds1):
+        one.share(me, p)
+    for p in range(first):
+        one.share_from(1, p)
 
     own_w1.wait()
-    for src in range(n):
-        @pl.when(src != me)
-        def _():
-            xy_landed(src).wait_recv()
 
     def up(p):
         for src in range(n):
@@ -298,27 +332,74 @@
                                      preferred_element_type=jnp.float32)
                 h[share, here, cols] = jnp.square(jnp.maximum(total, 0.0)).astype(jnp.bfloat16)
 
-    @pl.loop(0, max(rounds1 - 2, 0))
-    def _(p):
-        up(p)
-    if rounds1 > 1:
-        one.forward_near(rounds1 - 1)
-        for src in range(n):
-            one.share(src, rounds1 - 2)
-        up(rounds1 - 2)
-    for src in range(n):
-        one.share(src, rounds1 - 1)
-    up(rounds1 - 1)
+    def far(step, ends, p):
+        for o in range(2, n):
+            for src in (me - o, me + o):
+                end = (src == 0) | (src == n - 1)
+
+                @pl.when((src >= 0) & (src < n) & (end if ends else jnp.logical_not(end)))
+                def _():
+                    step(src, p)
+
+    def close(step, ends, p):
+        for src in (me - 1, me + 1):
+            end = (src == 0) | (src == n - 1) | (me == 0) | (me == n - 1)
+
+            @pl.when((src >= 0) & (src < n) & (end if ends else jnp.logical_not(end)))
+            def _():
+                step(src, p)
+
+    groups = [(close, True, p) for p in range(first, rounds1)]
+    groups += [(far, True, p) for p in range(rounds1)]
+    groups += [(close, False, p) for p in range(first, rounds1)]
+    groups += [(far, False, p) for p in range(rounds1)]
+    done = 0
+
+    def share_group(i):
+        which, ends, p = groups[i]
+        which(one.share, ends, p)
+
+    for i, (which, ends, p) in enumerate(groups):
+        which(one.forward, ends, p)
+        if i == min(rounds1, len(groups) - 1):
+            for src in range(n):
+                @pl.when(src != me)
+                def _():
+                    xy_landed(src).wait_recv()
+        if i >= lag_g:
+            share_group(i - lag_g)
+            after = i - lag_g - (len(groups) - rounds1)
+            if after >= 0 and i + 1 < len(groups):
+                up(after)
+                done = after + 1
+    ahead = jnp.where((me == 0) | (me == n - 1), min(lead, rounds2), min(lead_mid, rounds2))
+
+    def send_two(r):
+        @pl.when(r >= near)
+        def _():
+            two.send(r, 1, 1)
+        two.send(r, 2, n - 1)
+
+    @pl.loop(0, ahead)
+    def _(r):
+        send_two(r)
+    for i in range(max(len(groups) - lag_g, 0), len(groups)):
+        share_group(i)
+        after = i - (len(groups) - rounds1)
+        while done <= after:
+            up(done)
+            done += 1
     own_w2.wait()
 
     def where_of(t):
-        return t // n, lax.rem(t, n)
+        at = lax.rem(t + 4 * n * n, n)
+        return t // n, jnp.where(lax.rem(at, 2) == 0, at // 2, n - 1 - at // 2)
 
     def out_tile(ref, block, r):
-        return ref.at[at_rows(block * q, q), at_rows(r * tile, tile)]
+        return ref.at[at_rows(block * q, q), at_rows(r * tile2, tile2)]
 
     def down(start, d, r):
-        cols = at_rows(r * tile, tile)
+        cols = at_rows(r * tile2, tile2)
         here = at_rows(start, q)
         return (jnp.dot(h[0, here, :], w2s[0, d, :, cols], preferred_element_type=jnp.float32)
                 + jnp.dot(h[1, here, :], w2s[1, d, :, cols], preferred_element_type=jnp.float32))
@@ -360,13 +441,27 @@
         ref = st_recv.at[z, s]
         return remote(ref, ref, st_send.at[o, c], st_rcv.at[z, s], {"ra": z, "cb": s})
 
+    def source_of(t):
+        at = lax.rem(t, n)
+        return jnp.where(at < 2, at, n + 1 - at)
+
     def stage_r(t):
-        r, d = where_of(t)
-        two.forward(d, r)
+        o = source_of(t)
+
+        @pl.when(o > 0)
+        def _():
+            two.forward_from(o, t // n)
 
     def stage_x(t):
-        r, d = where_of(t)
-        two.share(d, r)
+        o = source_of(t)
+
+        @pl.when(o > 0)
+        def _():
+            two.share_from(o, t // n)
+
+        @pl.when(o == 0)
+        def _():
+            two.share(me, t // n)
 
     def stage_a(t):
         r, d = where_of(t)
@@ -405,11 +500,9 @@
         @pl.when(d == me)
         def _():
             out_tile(fin, slot_of(cb), r)[...] = acc[...].astype(jnp.bfloat16)
-            for o in range(1, m):
-                ag_copy(r, o).start()
             for c in range(qchunks):
                 sums = sums_of(acc[pl.ds(c * 128, 128), :] + residual_scale * xres[
-                    at_rows(slot_of(cb) * q + c * 128, 128), at_rows(r * tile, tile)].astype(
+                    at_rows(slot_of(cb) * q + c * 128, 128), at_rows(r * tile2, tile2)].astype(
                         jnp.float32))
                 st_src[pl.ds(c, 1), :] += sums[0:1, :]
                 st_src[pl.ds(qchunks + c, 1), :] += sums[64:65, :]
@@ -420,23 +513,30 @@
                     for c in range(m):
                         if o or c:
                             st_copy(o, c).start()
-
-    @pl.loop(0, tiles + lag_z + n - 1)
+            for o in range(1, m):
+                ag_copy(r, o).start()
+
+    def lag_of(hop):
+        return lag_z + hop * lag_hop + jnp.where(2 * hop >= n, lag_late, 0)
+
+    @pl.loop(0, tiles + lag_z + (n - 1) * lag_hop + lag_late)
     def _(step):
-        for r in range(lead, rounds2):
-            @pl.when(step == (r - lead + 1) * n)
-            def _():
-                two.send(r)
         for lag, stage in ((0, stage_r), (lag_x, stage_x), (lag_a, stage_a)):
             @pl.when((step >= lag) & (step < tiles + lag))
             def _():
                 stage(step - lag)
+            if stage is stage_r:
+                late = (step + 1) // n - 1 + ahead
+
+                @pl.when((lax.rem(step + 1, n) == 0) & (late < rounds2))
+                def _():
+                    send_two(late)
 
         @pl.loop(0, n)
         def _(back):
             hop = n - 1 - back
-            t = step - lag_z - hop
-            d = lax.rem(t + n * n, n)
+            t = step - lag_of(hop)
+            d = where_of(t)[1]
             mine = jnp.where(d > me, me, jnp.where(
                 d < me, n - 1 - me, jnp.maximum(me, n - 1 - me)))
 
@@ -502,7 +602,7 @@
 
     @pl.loop(0, tiles)
     def _(t):
-        d = lax.rem(t, n)
+        d = where_of(t)[1]
         y_copy(t).wait_send()
 
         @pl.when(d != me)
@@ -529,7 +629,8 @@
     assert m == 4 and nd == 2 and tokens % (128 * m) == 0 and tokens // m <= 512
     q = tokens // m
     tile = math.gcd(tile_cap, math.gcd(fs, dl))
-    rounds1, rounds2 = fs // tile, dl // tile
+    tile2 = math.gcd(tile2_cap, dl)
+    rounds1, rounds2 = fs // tile, dl // tile2
     tiles = rounds2 * n
     chunk_rows = -(-2 * (tokens // 128) // 8) * 8
     dma = pltpu.SemaphoreType.DMA
@@ -537,7 +638,7 @@
     hbm = pl.BlockSpec(memory_space=pl.ANY)
     vmem = pl.BlockSpec(memory_space=pltpu.VMEM)
     return pl.pallas_call(
-        functools.partial(kernel, n, m, tile),
+        functools.partial(kernel, n, m, tile, tile2),
         out_shape=jax.ShapeDtypeStruct((tokens, dl), bf16),
         in_specs=[hbm, hbm, hbm, hbm, vmem, vmem, vmem, vmem],
         out_specs=hbm,
@@ -555,12 +656,12 @@
             pltpu.VMEM((n * q, dl), bf16),
             pltpu.VMEM(((n + 1) * q, dl), bf16),
             pltpu.VMEM((tokens, dl), bf16),
-            pltpu.VMEM((q, tile), f32),
+            pltpu.VMEM((q, tile2), f32),
             pltpu.VMEM((8, 128), f32),
             pltpu.VMEM((n, m, 8, 128), f32),
             dma((4,)), dma((2, n)), dma((8, n, rounds1)), dma((8, n, rounds2)), dma((3, n)),
             dma((2, n)), dma((2, tiles)), dma((3, tiles)), dma((2, rounds2, m)), dma((n, m)),
-            dma((n, m)), dma((tokens // 128,)),
+            dma((n, m)), dma((tokens // 128,)), pltpu.SemaphoreType.REGULAR,
         ],
         compiler_params=pltpu.CompilerParams(
             collective_id=0, has_side_effects=True, vmem_limit_bytes=67 * 1000 * 1000),

time: 345 us -> 303 us (0.88)
  Pallas kernels: 337 us -> 298 us
    pallas_call x1, Pallas kernels: 337 us -> 298 us  [per_device(): pl.pallas_call(functools.partial(kernel, n, m, tile, tile2), out_shape=ja...]
where the time goes in v2:
time: 303 us; the launch traced here: 302 us
  Pallas kernels  298 us (98%)
  local copies, waits for them, and re-layouts  3.86 us (1%)
    pallas_call x1, Pallas kernels, per_device(): pl.pallas_call(functools.partial(kernel, n, m, tile, tile2), out_shape=ja...  298 us

profile of v2, /device:TPU:0, one launch (start us, length us, event | category | flops | bytes accessed | tf_op | source)
XLA Modules:
  0.0 301.7 jit_solution(2438538931031296621)
XLA Ops:
  0.0 297.9 %shard_map.82 = bf16[1536,1024]{1,0:T(8,128)(2,1)} custom-call(bf16[1536,1024]{1,0:T(8,128)(2,1)} %carried_hbm.1, bf16[1536,1024]{1,0:T(8,128)(2,1)} %branch_hbm.1, bf16[1024,4096]{1,0:T(8,128)(2,1)} %w1_hbm.1, bf16[4096,1024]{1,0:T(8,128)(2,1)} %w2_hbm.1, f32[1,1024]{1,0:T(1,128)} %bitcast.4, f32[1,1024]{1,0:T(1,128)} %bitcast.5, f32[1,1024]{1,0:T(1,128)} %bitcast.6, ...), custom_call_target="tpu_custom_call" | custom-call | tf_op jit(solution)/shard_map/pallas_call | solution.py:640
  297.9 3.9 %copy.10 = bf16[1536,1024]{1,0:T(8,128)(2,1)} copy(bf16[1536,1024]{1,0:T(8,128)(2,1)} %shard_map.82) | data formatting | bytes 6291456

commit v3 on v2

--- a/solution.py
+++ b/solution.py
@@ -12,7 +12,7 @@
 norm_eps = 1e-05
 tile_cap = 256
 tile2_cap = 128
-lag_x, lag_a, lag_z, lag_hop, lag_late = 3, 8, 14, 4, 12
+lag_x, lag_a, lag_z, lag_hop, lag_late = 3, 7, 14, 8, 0
 lead = 3
 lead_mid = 5
 near = 3
@@ -22,7 +22,7 @@
 
 def kernel(n, m, tile, tile2, carried_hbm, branch_hbm, w1_hbm, w2_hbm, gain_in_ref, bias_in_ref, gain_ref,
            bias_ref, o_hbm, s1_src, s1_recv, s1_tot, xh, xres, w1s, w2s, h, psend, yrecv, zsend,
-           zrecv, fin, acc, st_src, st_recv, loc_sem, s1_sem, w1_sem, w2_sem, xz_sem, xy_sem,
+           zrecv, fin, both, acc, st_src, st_recv, loc_sem, s1_sem, w1_sem, w2_sem, xz_sem, xy_sem,
            y_sem, z_sem, ag_sem, st_send, st_rcv, out_sem, meet_sem):
     me, cb, dp = lax.axis_index("ra"), lax.axis_index("cb"), lax.axis_index("dp")
     tokens, dl = xres.shape
@@ -343,7 +343,7 @@
 
     def close(step, ends, p):
         for src in (me - 1, me + 1):
-            end = (src == 0) | (src == n - 1) | (me == 0) | (me == n - 1)
+            end = (src == 0) | (src == n - 1)
 
             @pl.when((src >= 0) & (src < n) & (end if ends else jnp.logical_not(end)))
             def _():
@@ -398,11 +398,10 @@
     def out_tile(ref, block, r):
         return ref.at[at_rows(block * q, q), at_rows(r * tile2, tile2)]
 
-    def down(start, d, r):
+    def down(d, r):
         cols = at_rows(r * tile2, tile2)
-        here = at_rows(start, q)
-        return (jnp.dot(h[0, here, :], w2s[0, d, :, cols], preferred_element_type=jnp.float32)
-                + jnp.dot(h[1, here, :], w2s[1, d, :, cols], preferred_element_type=jnp.float32))
+        return (jnp.dot(h[0], w2s[0, d, :, cols], preferred_element_type=jnp.float32)
+                + jnp.dot(h[1], w2s[1, d, :, cols], preferred_element_type=jnp.float32))
 
     def y_copy(t):
         r, d = where_of(t)
@@ -423,14 +422,31 @@
         return remote(ref, ref, z_sem.at[0, t], z_sem.at[1 if to_right else 2, t], {
             "ra": jnp.maximum(me - 1, 0) if to_right else jnp.minimum(me + 1, n - 1)})
 
-    def ag_copy(r, o):
+    def ag_half(owner, half, r):
+        return fin.at[at_rows(slot_of(owner) * q + half * (q // 2), q // 2), at_rows(r * tile2, tile2)]
+
+    def ag_copy(r, side):
         ref = out_tile(fin, slot_of(cb), r)
-        return remote(ref, ref, ag_sem.at[0, r, o], ag_sem.at[1, r, cb], {"cb": lax.rem(cb + o, m)})
-
-    def ag_landed(r, o):
-        sender = lax.rem(cb + o, m)
-        ref = out_tile(fin, slot_of(sender), r)
-        return remote(ref, ref, ag_sem.at[0, r, o], ag_sem.at[1, r, sender], {"cb": sender})
+        return remote(ref, ref, ag_sem.at[0, r, side], ag_sem.at[1, r, side], {"cb": (px, py)[side]})
+
+    def ag_landed(r, side):
+        ref = out_tile(fin, slot_of((px, py)[side]), r)
+        return remote(ref, ref, ag_sem.at[0, r, side], ag_sem.at[1, r, side], {"cb": (px, py)[side]})
+
+    def ag_pass(r, side):
+        ref = ag_half((py, px)[side], 1 - side, r)
+        return remote(ref, ref, ag_sem.at[0, r, 2 + side], ag_sem.at[1, r, 2 + side], {
+            "cb": (px, py)[side]})
+
+    def ag_passed(r, side):
+        ref = ag_half(lax.rem(px + 2, m), 1 - side, r)
+        return remote(ref, ref, ag_sem.at[0, r, 2 + side], ag_sem.at[1, r, 2 + side], {
+            "cb": (px, py)[side]})
+
+    def relay_ag(r):
+        for side in range(2):
+            ag_landed(r, 1 - side).wait_recv()
+            ag_pass(r, side).start()
 
     def st_copy(o, c):
         return remote(st_src, st_recv.at[me, cb], st_send.at[o, c], st_rcv.at[me, cb],
@@ -466,14 +482,16 @@
     def stage_a(t):
         r, d = where_of(t)
         two.ready(d, r)
-        out_tile(psend, d, r)[...] = down((1 - yb) * q, d, r).astype(jnp.bfloat16)
+        both[...] = down(d, r)
+        out_tile(psend, d, r)[...] = both[at_rows((1 - yb) * q, q), :].astype(jnp.bfloat16)
         y_copy(t).start()
+        out_tile(zsend, d, r)[...] = both[at_rows(yb * q, q), :].astype(jnp.bfloat16)
 
     def stage_z(t):
         r, d = where_of(t)
-        acc[...] = down(yb * q, d, r)
         y_copy(t).wait_recv()
-        acc[...] += out_tile(yrecv, d, r)[...].astype(jnp.float32)
+        acc[...] = out_tile(zsend, d, r)[...].astype(jnp.float32) + out_tile(yrecv, d, r)[
+            ...].astype(jnp.float32)
 
         @pl.when((me >= 1) & (d >= me))
         def _():
@@ -513,8 +531,12 @@
                     for c in range(m):
                         if o or c:
                             st_copy(o, c).start()
-            for o in range(1, m):
-                ag_copy(r, o).start()
+            for side in range(2):
+                ag_copy(r, side).start()
+
+            @pl.when(r > 0)
+            def _():
+                relay_ag(r - 1)
 
     def lag_of(hop):
         return lag_z + hop * lag_hop + jnp.where(2 * hop >= n, lag_late, 0)
@@ -544,14 +566,49 @@
             def _():
                 stage_z(t)
 
+    relay_ag(rounds2 - 1)
+    for src in range(n):
+        @pl.when((src == me) | (src < me))
+        def _():
+            @pl.when(me + 1 < n)
+            def _():
+                xz(src, True).wait_send()
+
+        @pl.when((src == me) | (src > me))
+        def _():
+            @pl.when(me >= 1)
+            def _():
+                xz(src, False).wait_send()
+
+        @pl.when(src != me)
+        def _():
+            xy(src).wait_send()
+
+        for stream, count in ((one, rounds1), (two, rounds2)):
+            @pl.loop(0, count)
+            def _(p):
+                stream.sent(src, p)
+    for o in range(1, n):
+        s1_copy(o).wait_send()
+
+    @pl.loop(0, tiles)
+    def _(t):
+        d = where_of(t)[1]
+        y_copy(t).wait_send()
+
+        @pl.when(d != me)
+        def _():
+            z_copy(t, True).wait_send()
+
     for o in range(n):
         for c in range(m):
             if o or c:
                 st_landed(o, c).wait_recv()
     st_recv[me, cb] = st_src[...]
-    for o in range(1, m):
-        for r in range(rounds2):
-            ag_landed(r, o).wait_recv()
+    for side in range(2):
+        @pl.loop(0, rounds2)
+        def _(r):
+            ag_passed(r, side).wait_recv()
 
     def out_copy(c):
         here = at_rows(c * 128, 128)
@@ -569,49 +626,21 @@
             mean_row = s1_tot[pl.ds(c, 1), :] / width
             scale_row = lax.rsqrt(
                 s1_tot[pl.ds(qchunks + c, 1), :] / width - mean_row * mean_row + norm_eps)
-            here = at_rows(slot * q + c * 128, 128)
-            mixed = residual_scale * xres[here, :].astype(jnp.float32) + fin[here, :].astype(
-                jnp.float32)
-            xres[here, :] = ((mixed - column(mean_row)) * column(scale_row) * gain_ref[...]
-                             + bias_ref[...]).astype(jnp.bfloat16)
+            mean, scale = column(mean_row), column(scale_row)
+            for part in range(4):
+                here = at_rows(slot * q + c * 128 + part * 32, 32)
+                own = slice(part * 32, part * 32 + 32)
+                mixed = residual_scale * xres[here, :].astype(jnp.float32) + fin[here, :].astype(
+                    jnp.float32)
+                xres[here, :] = ((mixed - mean[own]) * scale[own] * gain_ref[...]
+                                 + bias_ref[...]).astype(jnp.bfloat16)
             out_copy(slot * qchunks + c).start()
 
-    for src in range(n):
-        @pl.when((src == me) | (src < me))
-        def _():
-            @pl.when(me + 1 < n)
-            def _():
-                xz(src, True).wait_send()
-
-        @pl.when((src == me) | (src > me))
-        def _():
-            @pl.when(me >= 1)
-            def _():
-                xz(src, False).wait_send()
-
-        @pl.when(src != me)
-        def _():
-            xy(src).wait_send()
-
-        for stream, count in ((one, rounds1), (two, rounds2)):
-            @pl.loop(0, count)
-            def _(p):
-                stream.sent(src, p)
-    for o in range(1, n):
-        s1_copy(o).wait_send()
-
-    @pl.loop(0, tiles)
-    def _(t):
-        d = where_of(t)[1]
-        y_copy(t).wait_send()
-
-        @pl.when(d != me)
-        def _():
-            z_copy(t, True).wait_send()
-
-    for o in range(1, m):
-        for r in range(rounds2):
-            ag_copy(r, o).wait_send()
+    for side in range(2):
+        @pl.loop(0, rounds2)
+        def _(r):
+            ag_copy(r, side).wait_send()
+            ag_pass(r, side).wait_send()
     for o in range(n):
         for c in range(m):
             if o or c:
@@ -656,6 +685,7 @@
             pltpu.VMEM((n * q, dl), bf16),
             pltpu.VMEM(((n + 1) * q, dl), bf16),
             pltpu.VMEM((tokens, dl), bf16),
+            pltpu.VMEM((2 * q, tile2), f32),
             pltpu.VMEM((q, tile2), f32),
             pltpu.VMEM((8, 128), f32),
             pltpu.VMEM((n, m, 8, 128), f32),

time: 303 us -> 293 us (0.967)
  Pallas kernels: 298 us -> 288 us
    pallas_call x1, Pallas kernels: 298 us -> 288 us  [per_device(): pl.pallas_call(functools.partial(kernel, n, m, tile, tile2), out_shape=ja...]
where the time goes in v3:
time: 293 us; the launch traced here: 292 us
  Pallas kernels  288 us (98%)
  local copies, waits for them, and re-layouts  3.86 us (1%)
    pallas_call x1, Pallas kernels, per_device(): pl.pallas_call(functools.partial(kernel, n, m, tile, tile2), out_shape=ja...  288 us

profile of v3, /device:TPU:0, one launch (start us, length us, event | category | flops | bytes accessed | tf_op | source)
XLA Modules:
  0.0 292.3 jit_solution(5251924923985561679)
XLA Ops:
  0.0 288.4 %shard_map.82 = bf16[1536,1024]{1,0:T(8,128)(2,1)} custom-call(bf16[1536,1024]{1,0:T(8,128)(2,1)} %carried_hbm.1, bf16[1536,1024]{1,0:T(8,128)(2,1)} %branch_hbm.1, bf16[1024,4096]{1,0:T(8,128)(2,1)} %w1_hbm.1, bf16[4096,1024]{1,0:T(8,128)(2,1)} %w2_hbm.1, f32[1,1024]{1,0:T(1,128)} %bitcast.4, f32[1,1024]{1,0:T(1,128)} %bitcast.5, f32[1,1024]{1,0:T(1,128)} %bitcast.6, ...), custom_call_target="tpu_custom_call" | custom-call | tf_op jit(solution)/shard_map/pallas_call | solution.py:669
  288.5 3.9 %copy.10 = bf16[1536,1024]{1,0:T(8,128)(2,1)} copy(bf16[1536,1024]{1,0:T(8,128)(2,1)} %shard_map.82) | data formatting | bytes 6291456

commit v4 on v3

--- a/solution.py
+++ b/solution.py
@@ -210,20 +210,24 @@
         s1_landed(o).wait_recv()
         s1_tot[...] += s1_recv[lax.rem(me + o, n)]
 
-    def normed(c):
+    def normed(c, local=None):
         mean_row = s1_tot[pl.ds(c, 1), :] / width
         scale_row = lax.rsqrt(s1_tot[pl.ds(chunks + c, 1), :] / width - mean_row * mean_row + norm_eps)
-        here = at_rows(c * 128, 128)
-        out = ((mixed_in(here) - column(mean_row)) * column(scale_row) * gain_in_ref[...]
-               + bias_in_ref[...]).astype(jnp.bfloat16)
-        xres[here, :] = out
-        return out
+        mean, scale = column(mean_row), column(scale_row)
+        for part in range(4):
+            here = at_rows(c * 128 + part * 32, 32)
+            own = slice(part * 32, part * 32 + 32)
+            out = ((mixed_in(here) - mean[own]) * scale[own] * gain_in_ref[...]
+                   + bias_in_ref[...]).astype(jnp.bfloat16)
+            xres[here, :] = out
+            if local is not None:
+                xh[me, at_rows(local * 128 + part * 32, 32), :] = out
 
     def normed_half(first, count):
         @pl.loop(0, count)
         def _(c):
             local = first + c
-            xh[me, at_rows(local * 128, 128), :] = normed(xb * 2 * qchunks + local)
+            normed(xb * 2 * qchunks + local, local)
 
     normed_half(yb * qchunks, qchunks)
 

time: 293 us -> 293 us (level)
  no operation moved by 1% of the time
where the time goes in v4:
time: 293 us; the launch traced here: 292 us
  Pallas kernels  288 us (98%)
  local copies, waits for them, and re-layouts  3.86 us (1%)
    pallas_call x1, Pallas kernels, per_device(): pl.pallas_call(functools.partial(kernel, n, m, tile, tile2), out_shape=ja...  288 us

profile of v4, /device:TPU:0, one launch (start us, length us, event | category | flops | bytes accessed | tf_op | source)
XLA Modules:
  0.0 292.3 jit_solution(16446699858465934382)
XLA Ops:
  0.0 288.4 %shard_map.82 = bf16[1536,1024]{1,0:T(8,128)(2,1)} custom-call(bf16[1536,1024]{1,0:T(8,128)(2,1)} %carried_hbm.1, bf16[1536,1024]{1,0:T(8,128)(2,1)} %branch_hbm.1, bf16[1024,4096]{1,0:T(8,128)(2,1)} %w1_hbm.1, bf16[4096,1024]{1,0:T(8,128)(2,1)} %w2_hbm.1, f32[1,1024]{1,0:T(1,128)} %bitcast.4, f32[1,1024]{1,0:T(1,128)} %bitcast.5, f32[1,1024]{1,0:T(1,128)} %bitcast.6, ...), custom_call_target="tpu_custom_call" | custom-call | tf_op jit(solution)/shard_map/pallas_call | solution.py:673
  288.5 3.9 %copy.10 = bf16[1536,1024]{1,0:T(8,128)(2,1)} copy(bf16[1536,1024]{1,0:T(8,128)(2,1)} %shard_map.82) | data formatting | bytes 6291456
